TPU v7x, 32 devices: a whole 2x2x4 slice. The times are simulated.
32 devices in a mesh: fs: 2 (over core), tp: 16 (over z, y, x).
Axes of the slice: x: 2, y: 2, z: 4, core: 2. Of those that a mesh axis runs over, the one named last changes fastest.
Arguments:
- trained_gate: float32 [16, 504, 2048], P(None, 'fs', 'tp'), may hold values from -0.125 to 0.125
- trained_up: float32 [16, 504, 2048], P(None, 'fs', 'tp'), may hold values from -0.125 to 0.125
- trained_down: float32 [16, 504, 2048], P(None, 'fs', 'tp'), may hold values from -0.25 to 0.25
- trained_shared_gate: float32 [504, 2048], P('fs', 'tp'), may hold values from -0.125 to 0.125
- trained_shared_up: float32 [504, 2048], P('fs', 'tp'), may hold values from -0.125 to 0.125
- trained_shared_down: float32 [504, 2048], P('fs', 'tp'), may hold values from -0.25 to 0.25
- ffn_gain: float32 [2048], P('tp'), may hold values from 0.1 to 1.9
- prompt_tokens: bfloat16 [512, 2048], P('fs'), may hold values from -6 to 6
- expert_ids: int32 [512, 8], P('fs'), may hold values from 0 to 15, all different within a row; in each aligned block of 256 rows (0 to 255, 256 to 511, ...) at most 256 rows name the same one
- route_scores: float32 [512, 8], P('fs'), may hold values from 0.05 to 1
Outputs:
- served_gate: bfloat16 [16, 504, 2048], P('tp')
- served_up: bfloat16 [16, 504, 2048], P('tp')
- served_down: bfloat16 [16, 504, 2048], P('tp')
- served_shared_gate: bfloat16 [504, 2048], P(None, 'tp')
- served_shared_up: bfloat16 [504, 2048], P(None, 'tp')
- served_shared_down: bfloat16 [504, 2048], P(None, 'tp')
- mixture_out: bfloat16 [512, 2048], P('fs', 'tp')
Inputs may be any that keep to these rules, and one draw needn't show every extreme that they name: `expert_ids`: each row names 8 different experts, and every expert is named by some row. Within the 256 rows of one index of fs no expert is named by more than 256 rows, and in every draw some expert is named by exactly 256 rows of some index of fs.
All inputs are finite; a program needn't handle non-finite values.
Results may differ from a plain program's by a relative error of at most 0.0082.
Values may be sent and summed in bfloat16 or wider, within the bound.
A program may use at most 64 MiB of HBM per device.

v0:
```python
import functools

import jax
import jax.numpy as jnp
from jax import lax
from jax.experimental import pallas as pl
from jax.experimental.pallas import tpu as pltpu
from jax.sharding import PartitionSpec as P

EPSILON = 1e-06
ROUTED_SCALE = 2.5


def contract(left, right):
    return lax.dot_general(
        left, right, (((1,), (1,)), ((), ())), preferred_element_type=jnp.float32
    )


def plain_on_device(
    trained_gate,
    trained_up,
    trained_down,
    trained_shared_gate,
    trained_shared_up,
    trained_shared_down,
    ffn_gain,
    prompt_tokens,
    expert_ids,
    route_scores,
):
    gate_cast = (trained_gate * ffn_gain[None, None, :]).astype(jnp.bfloat16)
    up_cast = (trained_up * ffn_gain[None, None, :]).astype(jnp.bfloat16)
    down_cast = trained_down.astype(jnp.bfloat16)
    shared_gate_cast = (trained_shared_gate * ffn_gain[None, :]).astype(jnp.bfloat16)[None]
    shared_up_cast = (trained_shared_up * ffn_gain[None, :]).astype(jnp.bfloat16)[None]
    shared_down_cast = trained_shared_down.astype(jnp.bfloat16)[None]
    expert_gate, expert_up, expert_down = (
        lax.all_to_all(gate_cast, "tp", split_axis=0, concat_axis=2, tiled=True),
        lax.all_to_all(up_cast, "tp", split_axis=0, concat_axis=2, tiled=True),
        lax.all_to_all(down_cast, "tp", split_axis=0, concat_axis=2, tiled=True),
    )
    token_count, model_width = prompt_tokens.shape
    tokens_float = prompt_tokens.astype(jnp.float32)
    normed = (
        tokens_float
        * lax.rsqrt(jnp.mean(tokens_float * tokens_float, axis=1, keepdims=True) + EPSILON)
    ).astype(jnp.bfloat16)
    column_width = ffn_gain.shape[0]
    expert_index = lax.axis_index("tp")
    normed_cols = lax.dynamic_slice_in_dim(normed, expert_index * column_width, column_width, 1)
    expert_count = lax.axis_size("tp")
    top_count = expert_ids.shape[1]
    capacity = min(token_count, 5 * token_count * top_count // (2 * expert_count))
    route_weight = ROUTED_SCALE * route_scores / jnp.sum(route_scores, axis=1, keepdims=True)
    chosen = expert_ids == expert_index
    present = jnp.any(chosen, axis=1)
    position = jnp.cumsum(present.astype(jnp.int32)) - 1
    slot_match = (position[None, :] == jnp.arange(capacity, dtype=jnp.int32)[:, None]) & present[
        None, :
    ]
    slot_token = jnp.sum(
        jnp.where(slot_match, jnp.arange(token_count, dtype=jnp.int32)[None, :], 0), axis=1
    )
    slot_rows = jnp.take(normed, slot_token, axis=0)
    gathered = (
        lax.all_gather(expert_gate, "fs", axis=1, tiled=True),
        lax.all_gather(expert_up, "fs", axis=1, tiled=True),
        lax.all_gather(expert_down, "fs", axis=1, tiled=True),
        lax.all_gather(shared_gate_cast, "fs", axis=1, tiled=True),
        lax.all_gather(shared_up_cast, "fs", axis=1, tiled=True),
        lax.all_gather(shared_down_cast, "fs", axis=1, tiled=True),
    )
    gate_full, up_full, down_full, sgate_full, sup_full, sdown_full = gathered
    gate_pre = contract(slot_rows, gate_full[0])
    up_pre = contract(slot_rows, up_full[0])
    sgate_part = contract(normed_cols, sgate_full[0])
    sup_part = contract(normed_cols, sup_full[0])
    expert_act = (jax.nn.silu(gate_pre) * up_pre).astype(jnp.bfloat16)
    shared_gate_pre, shared_up_pre = lax.psum((sgate_part, sup_part), "tp")
    shared_act = (jax.nn.silu(shared_gate_pre) * shared_up_pre).astype(jnp.bfloat16)
    expert_out = jnp.dot(expert_act, down_full[0], preferred_element_type=jnp.float32)
    shared_out = jnp.dot(shared_act, sdown_full[0], preferred_element_type=jnp.float32)
    arrived = lax.all_to_all(expert_out, "tp", split_axis=1, concat_axis=0, tiled=True)
    arrived = arrived.reshape(expert_count, capacity, column_width)

    def add_expert(total, inputs):
        source_index, source_rows = inputs
        source_chosen = expert_ids == source_index
        source_weight = jnp.sum(jnp.where(source_chosen, route_weight, 0.0), axis=1)
        source_present = jnp.any(source_chosen, axis=1)
        source_position = jnp.cumsum(source_present.astype(jnp.int32)) - 1
        source_picked = jnp.take(source_rows, jnp.maximum(source_position, 0), axis=0)
        return (
            total + jnp.where(source_present[:, None], source_picked * source_weight[:, None], 0.0),
            None,
        )

    routed_cols, _ = lax.scan(
        add_expert,
        jnp.zeros((token_count, column_width), jnp.float32),
        (jnp.arange(expert_count, dtype=jnp.int32), arrived),
    )
    mixture = (routed_cols + shared_out).astype(jnp.bfloat16)
    return (gate_full, up_full, down_full, sgate_full[0], sup_full[0], sdown_full[0], mixture)

TILE = 16
VMEM_BYTES = 67000000


def geometry(n, n_fs, experts, rows, columns):
    block = -(-rows // TILE) * TILE
    edge = block - rows
    if n_fs != 2 or experts != n or columns % 128 or n % 4 or not 0 < edge < 8 or block % (TILE * n):
        return None
    return block, edge, block // n


def far_first(count):
    return sorted(range(count), key=lambda step: -min(step, count - step))


def kernel(
    n,
    block,
    edge,
    piece,
    gate_in,
    up_in,
    down_in,
    sgate_in,
    sup_in,
    sdown_in,
    gain_in,
    tokens_in,
    ids_in,
    scores_in,
    gate_out,
    up_out,
    down_out,
    sgate_out,
    sup_out,
    sdown_out,
    mix_out,
    gain_ref,
    tokens_ref,
    ids_ref,
    scores_ref,
    raw,
    shared_raw,
    rim,
    shared_rim,
    packed,
    shared_half,
    held,
    normed,
    gate_acc,
    up_acc,
    act,
    parts,
    plane,
    line,
    total,
    mix,
    mix_sem,
    small_sem,
    load_sem,
    shared_load_sem,
    rim_send,
    rim_recv,
    shared_rim_send,
    shared_rim_recv,
    shared_send,
    shared_recv,
    shared_keep,
    send_sem,
    recv_sem,
    pass_send,
    pass_recv,
    keep_sem,
    plane_send,
    plane_recv,
    line_send,
    line_recv,
):
    routed_in = (gate_in, up_in, down_in)
    shared_in = (sgate_in, sup_in, sdown_in)
    routed_out = (gate_out, up_out, down_out)
    shared_out = (sgate_out, sup_out, sdown_out)
    me = lax.axis_index("tp")
    core = lax.axis_index("fs")
    other = 1 - core
    inner = 4
    outer = n // inner
    my_a, my_b = me // inner, me % inner
    rows, columns = sgate_in.shape
    chunks = 4 if rows % 4 == 0 else 1
    chunk = rows // chunks * n
    first = core == 0

    def load(m, at):
        here = pl.ds(at * chunk, chunk)
        return pltpu.make_async_copy(routed_in[m].at[here], raw.at[m, here], load_sem.at[m, at])

    def load_shared(m):
        return pltpu.make_async_copy(shared_in[m], shared_raw.at[m], shared_load_sem.at[m])

    def to_peer(m, dst):
        return pltpu.make_async_remote_copy(
            src_ref=packed.at[m, dst],
            dst_ref=held.at[m, me, core],
            send_sem=send_sem.at[m, dst],
            recv_sem=recv_sem.at[m, me],
            device_id={"tp": dst},
            device_id_type=pl.DeviceIdType.MESH,
        )

    def from_peer(m, src):
        return pltpu.make_async_remote_copy(
            src_ref=packed.at[m, src],
            dst_ref=held.at[m, src, core],
            send_sem=send_sem.at[m, src],
            recv_sem=recv_sem.at[m, src],
            device_id={"tp": src},
            device_id_type=pl.DeviceIdType.MESH,
        )

    def own(m):
        return pltpu.make_async_copy(packed.at[m, me], held.at[m, me, core], recv_sem.at[m, me])

    def to_core(m, src, half):
        return pltpu.make_async_remote_copy(
            src_ref=held.at[m, src, half],
            dst_ref=held.at[m, src, half],
            send_sem=pass_send.at[m, src],
            recv_sem=pass_recv.at[m, src],
            device_id={"fs": other},
            device_id_type=pl.DeviceIdType.MESH,
        )

    def keep(m, src, half):
        return pltpu.make_async_copy(
            held.at[m, src, half, pl.ds(0, block)],
            routed_out[m].at[
                pl.ds(half * block, block), pl.ds(pl.multiple_of(src * columns, 128), columns)
            ],
            keep_sem.at[m, src, half],
        )

    def rim_copy(m):
        return pltpu.make_async_remote_copy(
            src_ref=routed_in[m].at[pl.ds(0, edge * n)],
            dst_ref=rim.at[m],
            send_sem=rim_send.at[m],
            recv_sem=rim_recv.at[m],
            device_id={"fs": other},
            device_id_type=pl.DeviceIdType.MESH,
        )

    def shared_rim_copy(m):
        return pltpu.make_async_remote_copy(
            src_ref=shared_in[m].at[pl.ds(0, 8)],
            dst_ref=shared_rim.at[m],
            send_sem=shared_rim_send.at[m],
            recv_sem=shared_rim_recv.at[m],
            device_id={"fs": other},
            device_id_type=pl.DeviceIdType.MESH,
        )

    def shared_copy(m, half):
        return pltpu.make_async_remote_copy(
            src_ref=shared_half.at[m, half],
            dst_ref=shared_half.at[m, half],
            send_sem=shared_send.at[m],
            recv_sem=shared_recv.at[m],
            device_id={"fs": other},
            device_id_type=pl.DeviceIdType.MESH,
        )

    def keep_shared(m, half):
        return pltpu.make_async_copy(
            shared_half.at[m, half],
            shared_out[m].at[pl.ds(half * block, block)],
            shared_keep.at[m, half],
        )

    def to_plane(a, b):
        return pltpu.make_async_remote_copy(
            src_ref=parts.at[a, b],
            dst_ref=plane.at[my_b, a],
            send_sem=plane_send.at[a, b],
            recv_sem=plane_recv.at[my_b, a],
            device_id={"tp": my_a * inner + b},
            device_id_type=pl.DeviceIdType.MESH,
        )

    def from_plane(a, b):
        return pltpu.make_async_remote_copy(
            src_ref=parts.at[a, b],
            dst_ref=plane.at[b, a],
            send_sem=plane_send.at[a, b],
            recv_sem=plane_recv.at[b, a],
            device_id={"tp": my_a * inner + b},
            device_id_type=pl.DeviceIdType.MESH,
        )

    def to_line(a):
        return pltpu.make_async_remote_copy(
            src_ref=plane.at[my_b, a],
            dst_ref=line.at[my_a],
            send_sem=line_send.at[a],
            recv_sem=line_recv.at[my_a],
            device_id={"tp": a * inner + my_b},
            device_id_type=pl.DeviceIdType.MESH,
        )

    def from_line(a):
        return pltpu.make_async_remote_copy(
            src_ref=plane.at[my_b, a],
            dst_ref=line.at[a],
            send_sem=line_send.at[a],
            recv_sem=line_recv.at[a],
            device_id={"tp": a * inner + my_b},
            device_id_type=pl.DeviceIdType.MESH,
        )

    def assemble(value, tail):
        cut = block - TILE
        body = jnp.where(first, value[0:cut], value[edge : cut + edge])
        rest = jnp.where(
            first,
            jnp.concatenate([value[cut:rows], tail[0:edge]], axis=0),
            jnp.concatenate(
                [value[cut + edge : rows], jnp.zeros((2 * edge, columns), jnp.float32)], axis=0
            ),
        )
        return cut, body, rest

    smalls = [
        pltpu.make_async_copy(source, target, small_sem.at[at])
        for at, (source, target) in enumerate(
            (
                (gain_in, gain_ref),
                (tokens_in, tokens_ref),
                (ids_in, ids_ref),
                (scores_in, scores_ref),
            )
        )
    ]
    smalls[0].start()
    for m in range(3):
        load_shared(m).start()

    for m in range(3):
        for at in range(chunks):
            load(m, at).start()
    for copy in smalls[1:]:
        copy.start()

    barrier = pltpu.get_barrier_semaphore()
    pl.semaphore_signal(
        barrier, inc=1, device_id={"fs": other}, device_id_type=pl.DeviceIdType.MESH
    )

    def greet(step, carry):
        pl.semaphore_signal(
            barrier,
            inc=1,
            device_id={"tp": (me + step) % n},
            device_id_type=pl.DeviceIdType.MESH,
        )
        return carry

    lax.fori_loop(1, n, greet, 0)
    pl.semaphore_wait(barrier, n)

    for m in range(3):
        shared_rim_copy(m).start()
        rim_copy(m).start()
    smalls[0].wait()
    gain = gain_ref[...]
    for m in range(3):
        load_shared(m).wait()
        shared_rim_copy(m).wait()
        scale = gain if m < 2 else jnp.ones_like(gain)
        cut, body, rest = assemble(shared_raw[m], shared_rim[m])
        shared_half[m, core, 0:cut] = (body * scale).astype(jnp.bfloat16)
        shared_half[m, core, cut:block] = (rest * scale).astype(jnp.bfloat16)
    for m in range(3):
        rim_copy(m).wait()

    def pack(m, dst):
        scale = gain if m < 2 else jnp.ones_like(gain)
        cut = block - TILE
        start = dst + core * (edge * n)
        body = raw[m, pl.ds(start, cut, stride=n), :]
        end = raw[m, pl.ds(dst + cut * n, rows - cut, stride=n), :]
        head = rim[m, pl.ds(dst, edge, stride=n), :]
        rest = jnp.where(
            first,
            jnp.concatenate([end, head], axis=0),
            jnp.concatenate([end[edge:], jnp.zeros((2 * edge, columns), jnp.float32)], axis=0),
        )
        packed[m, dst, 0:cut] = (body * scale).astype(jnp.bfloat16)
        packed[m, dst, cut:block] = (rest * scale).astype(jnp.bfloat16)
        packed[m, dst, block : block + piece] = shared_half[
            m, core, pl.ds(pl.multiple_of(dst * piece, TILE), piece)
        ]

    outer_steps = far_first(outer)
    inner_steps = far_first(inner)

    def peer(da, db, sign):
        return ((my_a + sign * da + outer) % outer) * inner + (my_b + sign * db + inner) % inner

    for matrices in ((0, 1), (2,)):
        for m in matrices:
            for at in range(chunks):
                load(m, at).wait()
        for da in outer_steps:

            def send(db, carry):
                dst = peer(da, db, 1)
                for m in matrices:
                    pack(m, dst)
                    to_peer(m, dst).start()
                return carry

            lax.fori_loop(1 if da == 0 else 0, inner, send, 0)
    for m in range(3):
        pack(m, me)
        own(m).start()
        shared_copy(m, core).start()

    for copy in smalls[1:]:
        copy.wait()
    tokens = tokens_ref[...].astype(jnp.float32)
    mean = jnp.mean(tokens * tokens, axis=1, keepdims=True)
    scaled = (tokens * lax.rsqrt(mean + EPSILON)).astype(jnp.bfloat16)
    for i in range(n):
        normed[i] = scaled[:, i * columns : (i + 1) * columns]
    scores = scores_ref[...]
    weights = ROUTED_SCALE * scores / jnp.sum(scores, axis=0, keepdims=True)
    weight = jnp.sum(jnp.where(ids_ref[...] == me, weights, 0.0), axis=0, keepdims=True)
    weight = jnp.transpose(jnp.broadcast_to(weight, (8, weight.shape[1])))[:, 0:1]
    gate_acc[...] = jnp.zeros_like(gate_acc)
    up_acc[...] = jnp.zeros_like(up_acc)

    hidden = 2 * (block + piece)

    def arrive(m, src, local):
        if local:
            own(m).wait()
        else:
            from_peer(m, src).wait_recv()
        to_core(m, src, core).start()
        keep(m, src, core).start()

    def complete(m, src):
        to_core(m, src, other).wait_recv()
        keep(m, src, other).start()
        return held[m, src].reshape(hidden, columns)

    def add(src):
        for m, acc in ((0, gate_acc), (1, up_acc)):
            acc[...] += lax.dot_general(
                normed[src],
                complete(m, src),
                (((1,), (1,)), ((), ())),
                preferred_element_type=jnp.float32,
            )

    def stream(matrices, use, after_group):
        for m in matrices:
            arrive(m, me, True)
        before = me
        for at, da in enumerate(outer_steps):

            def one(db, waiting):
                src = peer(da, (db + 1) % inner, -1)
                for m in matrices:
                    arrive(m, src, False)
                use(waiting)
                return src

            before = lax.fori_loop(0, inner - 1 if da == 0 else inner, one, before)
            after_group(at)
        use(before)

    stream((0, 1), add, lambda at: None)

    gate_pre = gate_acc[...]
    place = lax.broadcasted_iota(jnp.int32, gate_pre.shape, 1) % (block + piece)
    share = jnp.where(place < block, weight, 1.0)
    act[...] = (gate_pre / (1.0 + jnp.exp(-gate_pre)) * up_acc[...] * share).astype(jnp.bfloat16)

    def part(src):
        a, b = src // inner, src % inner
        parts[a, b] = jnp.dot(
            act[...], complete(2, src), preferred_element_type=jnp.float32
        ).astype(jnp.bfloat16)

        @pl.when(b != my_b)
        def _():
            to_plane(a, b).start()

    def plane_sum(a):
        result = parts[a, my_b].astype(jnp.float32)
        for db in range(1, inner):
            b = (my_b + db) % inner
            from_plane(a, b).wait_recv()
            result = result + plane[b, a].astype(jnp.float32)
        return result

    def flush(da):
        a = (my_a - da + outer) % outer
        plane[my_b, a] = plane_sum(a).astype(jnp.bfloat16)
        to_line(a).start()

    def after_group(at):
        if at > 0:
            flush(outer_steps[at - 1])

    stream((2,), part, after_group)
    total[...] = plane_sum(my_a)
    for m in range(3):
        shared_copy(m, other).wait_recv()
        for half in range(2):
            keep_shared(m, half).start()
    for da in range(1, outer):
        a = (my_a + da) % outer
        from_line(a).wait_recv()
        total[...] += line[a].astype(jnp.float32)
    mix[...] = total[...].astype(jnp.bfloat16)
    put_mix = pltpu.make_async_copy(mix, mix_out, mix_sem)
    put_mix.start()
    put_mix.wait()

    def drain(src, carry):
        for m in range(3):
            to_core(m, src, core).wait_send()
            keep(m, src, 0).wait()
            keep(m, src, 1).wait()
        return carry

    lax.fori_loop(0, n, drain, 0)

    def drain_sends(step, carry):
        for m in range(3):
            to_peer(m, (me + step) % n).wait_send()
        return carry

    lax.fori_loop(1, n, drain_sends, 0)
    for m in range(3):
        shared_copy(m, core).wait_send()
        for half in range(2):
            keep_shared(m, half).wait()
    for da in range(outer):
        a = (my_a + da) % outer
        for db in range(1, inner):
            to_plane(a, (my_b + db) % inner).wait_send()
        if da:
            to_line(a).wait_send()


def trim(count, pieces, *refs):
    sources, targets, rooms = refs[:count], refs[count : 2 * count], refs[2 * count : 3 * count]
    load_sem, store_sem = refs[3 * count :]
    loads, stores = [], []
    for at in range(count):
        rows = sources[at].shape[0]
        left = targets[at].shape[0]
        size = rows // pieces
        for step in range(pieces):
            here = pl.ds(step * size, size)
            there = pl.ds(step * size, min(size, left - step * size))
            loads.append(
                pltpu.make_async_copy(
                    sources[at].at[here], rooms[at].at[here], load_sem.at[at, step]
                )
            )
            stores.append(
                pltpu.make_async_copy(
                    rooms[at].at[there], targets[at].at[there], store_sem.at[at, step]
                )
            )
    for load in loads:
        load.start()
    for load, store in zip(loads, stores):
        load.wait()
        store.start()
    for store in stores:
        store.wait()


def on_device(n, shape, gate, up, down, sgate, sup, sdown, gain, tokens, ids, scores):
    block, edge, piece = shape
    experts, rows, columns = gate.shape
    count, width = tokens.shape
    hidden = 2 * (block + piece)
    inner, outer = 4, n // 4
    sem = pltpu.SemaphoreType.DMA
    anywhere = pl.BlockSpec(memory_space=pl.ANY)
    hbm = pl.BlockSpec(memory_space=pltpu.HBM)
    vmem = pl.BlockSpec(memory_space=pltpu.VMEM)
    bf16, f32 = jnp.bfloat16, jnp.float32
    full = jax.ShapeDtypeStruct((2 * block, width), bf16)
    thin = jax.ShapeDtypeStruct((2 * block, columns), bf16)
    results = pl.pallas_call(
        functools.partial(kernel, n, block, edge, piece),
        out_shape=(full, full, full, thin, thin, thin, jax.ShapeDtypeStruct((count, columns), bf16)),
        in_specs=[hbm] * 10,
        out_specs=(anywhere,) * 7,
        scratch_shapes=[
            pltpu.VMEM((1, columns), f32),
            pltpu.VMEM(tokens.shape, bf16),
            pltpu.VMEM(ids.shape[::-1], jnp.int32),
            pltpu.VMEM(scores.shape[::-1], f32),
            pltpu.VMEM((3, n * rows, columns), f32),
            pltpu.VMEM((3, rows, columns), f32),
            pltpu.VMEM((3, n * edge, columns), f32),
            pltpu.VMEM((3, 8, columns), f32),
            pltpu.VMEM((3, n, block + piece, columns), bf16),
            pltpu.VMEM((3, 2, block, columns), bf16),
            pltpu.VMEM((3, n, 2, block + piece, columns), bf16),
            pltpu.VMEM((n, count, columns), bf16),
            pltpu.VMEM((count, hidden), f32),
            pltpu.VMEM((count, hidden), f32),
            pltpu.VMEM((count, hidden), bf16),
            pltpu.VMEM((outer, inner, count, columns), bf16),
            pltpu.VMEM((inner, outer, count, columns), bf16),
            pltpu.VMEM((outer, count, columns), bf16),
            pltpu.VMEM((count, columns), f32),
            pltpu.VMEM((count, columns), bf16),
            sem,
            sem((4,)),
            sem((3, n)),
            sem((3,)),
            sem((3,)),
            sem((3,)),
            sem((3,)),
            sem((3,)),
            sem((3,)),
            sem((3,)),
            sem((3, 2)),
            sem((3, n)),
            sem((3, n)),
            sem((3, n)),
            sem((3, n)),
            sem((3, n, 2)),
            sem((outer, inner)),
            sem((inner, outer)),
            sem((outer,)),
            sem((outer,)),
        ],
        compiler_params=pltpu.CompilerParams(
            collective_id=0, has_side_effects=True, vmem_limit_bytes=VMEM_BYTES
        ),
    )(
        *[jnp.transpose(array, (1, 0, 2)).reshape(rows * n, columns) for array in (gate, up, down)],
        sgate,
        sup,
        sdown,
        gain[None, :],
        tokens,
        ids.T,
        scores.T,
    )
    pieces = 2
    whole = pl.pallas_call(
        functools.partial(trim, len(results), pieces),
        out_shape=tuple(
            jax.ShapeDtypeStruct((min(2 * rows, array.shape[0]), array.shape[1]), bf16)
            for array in results
        ),
        in_specs=[anywhere] * len(results),
        out_specs=(hbm,) * len(results),
        scratch_shapes=[pltpu.VMEM(array.shape, bf16) for array in results]
        + [sem((len(results), pieces))] * 2,
        compiler_params=pltpu.CompilerParams(vmem_limit_bytes=VMEM_BYTES),
    )(*results)
    return (*[array[None] for array in whole[:3]], *whole[3:])


def body(n, n_fs, *args):
    experts, rows, columns = args[0].shape
    shape = geometry(n, n_fs, experts, rows, columns)
    if shape is None:
        return plain_on_device(*args)
    return on_device(n, shape, *args)


def solution(mesh):
    placed = (
        P(None, "fs", "tp"),
        P(None, "fs", "tp"),
        P(None, "fs", "tp"),
        P("fs", "tp"),
        P("fs", "tp"),
        P("fs", "tp"),
        P("tp"),
        P("fs", None),
        P("fs", None),
        P("fs", None),
    )
    return jax.shard_map(
        functools.partial(body, mesh.shape["tp"], mesh.shape["fs"]),
        mesh=mesh,
        in_specs=placed,
        out_specs=(
            P("tp", None, None),
            P("tp", None, None),
            P("tp", None, None),
            P(None, "tp"),
            P(None, "tp"),
            P(None, "tp"),
            P("fs", "tp"),
        ),
        check_vma=False,
    )
```

profile of v0, /device:TPU:8, one launch (start us, length us, event | category | flops | bytes accessed | tf_op | source)
XLA Modules:
  0.0 103.7 jit_solution(15840059615765627011)
XLA Ops:
  0.6 97.3 %shard_map.153 = (bf16[512,2048]{1,0:T(8,128)(2,1)}, bf16[512,2048]{1,0:T(8,128)(2,1)}, bf16[512,2048]{1,0:T(8,128)(2,1)}, bf16[512,128]{1,0:T(8,128)(2,1)}, bf1...) custom-call(f32[4032,128]{1,0:T(8,128)} %bitcast.15, f32[4032,128]{1,0:T(8,128)} %bitcast.16, ...), custom_call_target="tpu_custom_call" | custom-call | tf_op jit(solution)/shard_map/pallas_call | solution.py:609
  98.0 5.7 %shard_map.154 = (bf16[504,2048]{1,0:T(8,128)(2,1)}, bf16[504,2048]{1,0:T(8,128)(2,1)}, bf16[504,2048]{1,0:T(8,128)(2,1)}, bf16[504,128]{1,0:T(8,128)(2,1)}, bf1...) custom-call(bf16[512,2048]{1,0:T(8,128)(2,1)} %get-tuple-element.21.refs_0_, ...), custom_call_target="tpu_custom_call" | custom-call | tf_op jit(solution)/shard_map/pallas_call | solution.py:670
where the time goes:
time: 105 us; the launch traced here: 104 us
  Pallas kernels  103 us (98%)
    pallas_call x1, Pallas kernels, on_device(): pl.pallas_call(functools.partial(kernel, n, block, edge, piece), out_shap...  97.3 us
    pallas_call x1, Pallas kernels, on_device(): pl.pallas_call(functools.partial(trim, len(results), pieces), out_shape=t...  5.7 us

commit v1 on v0

--- a/solution.py
+++ b/solution.py
@@ -113,11 +113,9 @@
     edge = block - rows
     if n_fs != 2 or experts != n or columns % 128 or n % 4 or not 0 < edge < 8 or block % (TILE * n):
         return None
+    if n // 4 != 4:
+        return None
     return block, edge, block // n
-
-
-def far_first(count):
-    return sorted(range(count), key=lambda step: -min(step, count - step))
 
 
 def kernel(
@@ -249,7 +247,7 @@
 
     def rim_copy(m):
         return pltpu.make_async_remote_copy(
-            src_ref=routed_in[m].at[pl.ds(0, edge * n)],
+            src_ref=raw.at[m, pl.ds(0, edge * n)],
             dst_ref=rim.at[m],
             send_sem=rim_send.at[m],
             recv_sem=rim_recv.at[m],
@@ -259,7 +257,7 @@
 
     def shared_rim_copy(m):
         return pltpu.make_async_remote_copy(
-            src_ref=shared_in[m].at[pl.ds(0, 8)],
+            src_ref=shared_raw.at[m, pl.ds(0, 8)],
             dst_ref=shared_rim.at[m],
             send_sem=shared_rim_send.at[m],
             recv_sem=shared_rim_recv.at[m],
@@ -372,22 +370,33 @@
         return carry
 
     lax.fori_loop(1, n, greet, 0)
+    smalls[0].wait()
+    for m in range(3):
+        load_shared(m).wait()
+    for m in range(2):
+        for at in range(chunks):
+            load(m, at).wait()
+    load(2, 0).wait()
     pl.semaphore_wait(barrier, n)
 
-    for m in range(3):
-        shared_rim_copy(m).start()
-        rim_copy(m).start()
-    smalls[0].wait()
+    @pl.when(core == 1)
+    def _():
+        for m in range(3):
+            shared_rim_copy(m).start()
+            rim_copy(m).start()
+
+    @pl.when(core == 0)
+    def _():
+        for m in range(3):
+            shared_rim_copy(m).wait_recv()
+            rim_copy(m).wait_recv()
+
     gain = gain_ref[...]
     for m in range(3):
-        load_shared(m).wait()
-        shared_rim_copy(m).wait()
         scale = gain if m < 2 else jnp.ones_like(gain)
         cut, body, rest = assemble(shared_raw[m], shared_rim[m])
         shared_half[m, core, 0:cut] = (body * scale).astype(jnp.bfloat16)
         shared_half[m, core, cut:block] = (rest * scale).astype(jnp.bfloat16)
-    for m in range(3):
-        rim_copy(m).wait()
 
     def pack(m, dst):
         scale = gain if m < 2 else jnp.ones_like(gain)
@@ -407,26 +416,71 @@
             m, core, pl.ds(pl.multiple_of(dst * piece, TILE), piece)
         ]
 
-    outer_steps = far_first(outer)
-    inner_steps = far_first(inner)
-
-    def peer(da, db, sign):
-        return ((my_a + sign * da + outer) % outer) * inner + (my_b + sign * db + inner) % inner
-
-    for matrices in ((0, 1), (2,)):
-        for m in matrices:
-            for at in range(chunks):
-                load(m, at).wait()
-        for da in outer_steps:
-
-            def send(db, carry):
-                dst = peer(da, db, 1)
-                for m in matrices:
-                    pack(m, dst)
+    mirror = outer - 1 - my_a
+    skip = (my_a + outer // 2) % outer
+    beside = my_a + 1 - 2 * (my_a % 2)
+    edge_plane = ((my_a + 1) // 2 + 1) % 2
+    inner_plane = 1 - edge_plane
+    third = edge_plane * mirror + inner_plane * skip
+    fourth = edge_plane * skip + inner_plane * mirror
+
+    def place_of(step, rising):
+        turn = step + rising * (inner - 1 - 2 * step)
+        return (2 * turn + 1 - turn // 2) % inner
+
+    def member(plane_at, shift):
+        column = (my_b + shift) % 2 + 2 * ((my_b // 2 + shift // 2) % 2)
+        return plane_at * inner + column
+
+    def peer_to(plane_at, step):
+        return member(plane_at, place_of(step, (plane_at > my_a).astype(jnp.int32)))
+
+    def peer_from(plane_at, step):
+        return member(plane_at, place_of(step, (plane_at < my_a).astype(jnp.int32)))
+
+    def send_plane(matrices, plane_at, start):
+        def send(step, carry):
+            dst = peer_to(plane_at, step)
+            for m in matrices:
+                pack(m, dst)
+                if start:
                     to_peer(m, dst).start()
-                return carry
-
-            lax.fori_loop(1 if da == 0 else 0, inner, send, 0)
+            return carry
+
+        lax.fori_loop(0, inner, send, 0)
+
+    def send_own(matrices):
+        def send(step, carry):
+            dst = member(my_a, step)
+            for m in matrices:
+                pack(m, dst)
+                to_peer(m, dst).start()
+            return carry
+
+        lax.fori_loop(1, inner, send, 0)
+
+    def launch(m, plane_at):
+        def send(step, carry):
+            to_peer(m, peer_to(plane_at, step)).start()
+            return carry
+
+        lax.fori_loop(0, inner, send, 0)
+
+    for plane_at in (mirror, skip, beside):
+        send_plane((0, 1), plane_at, True)
+    send_own((0, 1))
+    for at in range(1, chunks):
+        load(2, at).wait()
+    send_plane((2,), beside, True)
+    send_own((2,))
+    for plane_at in (skip, mirror):
+        send_plane((2,), plane_at, False)
+
+    @pl.when(inner_plane == 1)
+    def _():
+        launch(2, skip)
+        launch(2, mirror)
+
     for m in range(3):
         pack(m, me)
         own(m).start()
@@ -470,24 +524,29 @@
                 preferred_element_type=jnp.float32,
             )
 
-    def stream(matrices, use, after_group):
+    def stream(matrices, use, planes, after_group):
         for m in matrices:
             arrive(m, me, True)
         before = me
-        for at, da in enumerate(outer_steps):
-
-            def one(db, waiting):
-                src = peer(da, (db + 1) % inner, -1)
+        for at, plane_at in enumerate((my_a,) + planes):
+
+            def one(step, waiting):
+                src = member(my_a, step) if at == 0 else peer_from(plane_at, step)
                 for m in matrices:
                     arrive(m, src, False)
                 use(waiting)
                 return src
 
-            before = lax.fori_loop(0, inner - 1 if da == 0 else inner, one, before)
+            before = lax.fori_loop(1 if at == 0 else 0, inner, one, before)
             after_group(at)
         use(before)
 
-    stream((0, 1), add, lambda at: None)
+    stream((0, 1), add, (third, beside, fourth), lambda at: None)
+
+    @pl.when(edge_plane == 1)
+    def _():
+        launch(2, mirror)
+        launch(2, skip)
 
     gate_pre = gate_acc[...]
     place = lax.broadcasted_iota(jnp.int32, gate_pre.shape, 1) % (block + piece)
@@ -512,17 +571,20 @@
             result = result + plane[b, a].astype(jnp.float32)
         return result
 
-    def flush(da):
-        a = (my_a - da + outer) % outer
+    def flush(a):
         plane[my_b, a] = plane_sum(a).astype(jnp.bfloat16)
         to_line(a).start()
 
+    down_planes = (beside, third, fourth)
+
     def after_group(at):
-        if at > 0:
-            flush(outer_steps[at - 1])
-
-    stream((2,), part, after_group)
-    total[...] = plane_sum(my_a)
+        if at == 1:
+            total[...] = plane_sum(my_a)
+        if at > 1:
+            flush(down_planes[at - 2])
+
+    stream((2,), part, down_planes, after_group)
+    flush(fourth)
     for m in range(3):
         shared_copy(m, other).wait_recv()
         for half in range(2):
@@ -551,6 +613,13 @@
         return carry
 
     lax.fori_loop(1, n, drain_sends, 0)
+
+    @pl.when(core == 1)
+    def _():
+        for m in range(3):
+            shared_rim_copy(m).wait_send()
+            rim_copy(m).wait_send()
+
     for m in range(3):
         shared_copy(m, core).wait_send()
         for half in range(2):

time: 105 us -> 99.5 us (0.948); the launches traced: 104 us -> 99.4 us
  Pallas kernels: 103 us -> 98.7 us
    pallas_call x1, Pallas kernels: 97.3 us -> 93 us  [on_device(): pl.pallas_call(functools.partial(kernel, n, block, edge, piece), out_shap...]
where the time goes in v1:
time: 99.5 us; the launch traced here: 99.4 us
  Pallas kernels  98.7 us (99%)
    pallas_call x1, Pallas kernels, on_device(): pl.pallas_call(functools.partial(kernel, n, block, edge, piece), out_shap...  93 us
    pallas_call x1, Pallas kernels, on_device(): pl.pallas_call(functools.partial(trim, len(results), pieces), out_shape=t...  5.7 us

profile of v1, /device:TPU:8, one launch (start us, length us, event | category | flops | bytes accessed | tf_op | source)
XLA Modules:
  0.0 99.4 jit_solution(2970744067584314728)
XLA Ops:
  0.6 93.0 %shard_map.153 = (bf16[512,2048]{1,0:T(8,128)(2,1)}, bf16[512,2048]{1,0:T(8,128)(2,1)}, bf16[512,2048]{1,0:T(8,128)(2,1)}, bf16[512,128]{1,0:T(8,128)(2,1)}, bf1...) custom-call(f32[4032,128]{1,0:T(8,128)} %bitcast.15, f32[4032,128]{1,0:T(8,128)} %bitcast.16, ...), custom_call_target="tpu_custom_call" | custom-call | tf_op jit(solution)/shard_map/pallas_call | solution.py:678
  93.7 5.7 %shard_map.154 = (bf16[504,2048]{1,0:T(8,128)(2,1)}, bf16[504,2048]{1,0:T(8,128)(2,1)}, bf16[504,2048]{1,0:T(8,128)(2,1)}, bf16[504,128]{1,0:T(8,128)(2,1)}, bf1...) custom-call(bf16[512,2048]{1,0:T(8,128)(2,1)} %get-tuple-element.21.refs_0_, ...), custom_call_target="tpu_custom_call" | custom-call | tf_op jit(solution)/shard_map/pallas_call | solution.py:739

commit v2 on v1

v2 whole, which is shorter than its diff:
```python
import functools

import jax
import jax.numpy as jnp
from jax import lax
from jax.experimental import pallas as pl
from jax.experimental.pallas import tpu as pltpu
from jax.sharding import PartitionSpec as P

EPSILON = 1e-06
ROUTED_SCALE = 2.5


def contract(left, right):
    return lax.dot_general(
        left, right, (((1,), (1,)), ((), ())), preferred_element_type=jnp.float32
    )


def plain_on_device(
    trained_gate,
    trained_up,
    trained_down,
    trained_shared_gate,
    trained_shared_up,
    trained_shared_down,
    ffn_gain,
    prompt_tokens,
    expert_ids,
    route_scores,
):
    gate_cast = (trained_gate * ffn_gain[None, None, :]).astype(jnp.bfloat16)
    up_cast = (trained_up * ffn_gain[None, None, :]).astype(jnp.bfloat16)
    down_cast = trained_down.astype(jnp.bfloat16)
    shared_gate_cast = (trained_shared_gate * ffn_gain[None, :]).astype(jnp.bfloat16)[None]
    shared_up_cast = (trained_shared_up * ffn_gain[None, :]).astype(jnp.bfloat16)[None]
    shared_down_cast = trained_shared_down.astype(jnp.bfloat16)[None]
    expert_gate, expert_up, expert_down = (
        lax.all_to_all(gate_cast, "tp", split_axis=0, concat_axis=2, tiled=True),
        lax.all_to_all(up_cast, "tp", split_axis=0, concat_axis=2, tiled=True),
        lax.all_to_all(down_cast, "tp", split_axis=0, concat_axis=2, tiled=True),
    )
    token_count, model_width = prompt_tokens.shape
    tokens_float = prompt_tokens.astype(jnp.float32)
    normed = (
        tokens_float
        * lax.rsqrt(jnp.mean(tokens_float * tokens_float, axis=1, keepdims=True) + EPSILON)
    ).astype(jnp.bfloat16)
    column_width = ffn_gain.shape[0]
    expert_index = lax.axis_index("tp")
    normed_cols = lax.dynamic_slice_in_dim(normed, expert_index * column_width, column_width, 1)
    expert_count = lax.axis_size("tp")
    top_count = expert_ids.shape[1]
    capacity = min(token_count, 5 * token_count * top_count // (2 * expert_count))
    route_weight = ROUTED_SCALE * route_scores / jnp.sum(route_scores, axis=1, keepdims=True)
    chosen = expert_ids == expert_index
    present = jnp.any(chosen, axis=1)
    position = jnp.cumsum(present.astype(jnp.int32)) - 1
    slot_match = (position[None, :] == jnp.arange(capacity, dtype=jnp.int32)[:, None]) & present[
        None, :
    ]
    slot_token = jnp.sum(
        jnp.where(slot_match, jnp.arange(token_count, dtype=jnp.int32)[None, :], 0), axis=1
    )
    slot_rows = jnp.take(normed, slot_token, axis=0)
    gathered = (
        lax.all_gather(expert_gate, "fs", axis=1, tiled=True),
        lax.all_gather(expert_up, "fs", axis=1, tiled=True),
        lax.all_gather(expert_down, "fs", axis=1, tiled=True),
        lax.all_gather(shared_gate_cast, "fs", axis=1, tiled=True),
        lax.all_gather(shared_up_cast, "fs", axis=1, tiled=True),
        lax.all_gather(shared_down_cast, "fs", axis=1, tiled=True),
    )
    gate_full, up_full, down_full, sgate_full, sup_full, sdown_full = gathered
    gate_pre = contract(slot_rows, gate_full[0])
    up_pre = contract(slot_rows, up_full[0])
    sgate_part = contract(normed_cols, sgate_full[0])
    sup_part = contract(normed_cols, sup_full[0])
    expert_act = (jax.nn.silu(gate_pre) * up_pre).astype(jnp.bfloat16)
    shared_gate_pre, shared_up_pre = lax.psum((sgate_part, sup_part), "tp")
    shared_act = (jax.nn.silu(shared_gate_pre) * shared_up_pre).astype(jnp.bfloat16)
    expert_out = jnp.dot(expert_act, down_full[0], preferred_element_type=jnp.float32)
    shared_out = jnp.dot(shared_act, sdown_full[0], preferred_element_type=jnp.float32)
    arrived = lax.all_to_all(expert_out, "tp", split_axis=1, concat_axis=0, tiled=True)
    arrived = arrived.reshape(expert_count, capacity, column_width)

    def add_expert(total, inputs):
        source_index, source_rows = inputs
        source_chosen = expert_ids == source_index
        source_weight = jnp.sum(jnp.where(source_chosen, route_weight, 0.0), axis=1)
        source_present = jnp.any(source_chosen, axis=1)
        source_position = jnp.cumsum(source_present.astype(jnp.int32)) - 1
        source_picked = jnp.take(source_rows, jnp.maximum(source_position, 0), axis=0)
        return (
            total + jnp.where(source_present[:, None], source_picked * source_weight[:, None], 0.0),
            None,
        )

    routed_cols, _ = lax.scan(
        add_expert,
        jnp.zeros((token_count, column_width), jnp.float32),
        (jnp.arange(expert_count, dtype=jnp.int32), arrived),
    )
    mixture = (routed_cols + shared_out).astype(jnp.bfloat16)
    return (gate_full, up_full, down_full, sgate_full[0], sup_full[0], sdown_full[0], mixture)

TILE = 16
INNER = 4
VMEM_BYTES = 40000000


def geometry(n, n_fs, experts, rows, columns):
    block = -(-rows // TILE) * TILE
    edge = block - rows
    if n_fs != 2 or experts != n or columns % 128 or not 0 < edge < 8 or block % (TILE * n):
        return None
    if n != INNER * INNER or rows % INNER:
        return None
    return block, edge, block // n


def kernel(
    n,
    block,
    edge,
    piece,
    gate_in,
    up_in,
    down_in,
    sgate_in,
    sup_in,
    sdown_in,
    gain_in,
    tokens_in,
    ids_in,
    scores_in,
    held_pre,
    held_down,
    shared_half,
    mix,
    gain_ref,
    tokens_ref,
    ids_ref,
    scores_ref,
    raw,
    shared_raw,
    rim,
    shared_rim,
    packed_pre,
    packed_down,
    normed,
    gate_acc,
    up_acc,
    act,
    parts,
    plane,
    summed,
    stage,
    relay,
    line,
    small_sem,
    load_sem,
    shared_load_sem,
    rim_sem,
    shared_sem,
    send_sem,
    recv_sem,
    pass_send,
    pass_recv,
    plane_send,
    plane_recv,
    line_send,
    line_recv,
    relay_recv,
):
    routed_in = (gate_in, up_in, down_in)
    shared_in = (sgate_in, sup_in, sdown_in)
    packed = (packed_pre, packed_down)
    held = (held_pre, held_down)
    me = lax.axis_index("tp")
    core = lax.axis_index("fs")
    other = 1 - core
    inner = INNER
    outer = n // inner
    my_a, my_b = me // inner, me % inner
    rows, columns = sgate_in.shape
    chunks = INNER
    chunk = rows // chunks * n
    first = core == 0

    mirror = outer - 1 - my_a
    skip = (my_a + outer // 2) % outer
    beside = my_a + 1 - 2 * (my_a % 2)
    edge_plane = ((my_a + 1) // 2 + 1) % 2
    inner_plane = 1 - edge_plane
    third = edge_plane * mirror + inner_plane * skip
    fourth = edge_plane * skip + inner_plane * mirror

    def mesh_copy(source, target, send, recv, device):
        return pltpu.make_async_remote_copy(
            src_ref=source,
            dst_ref=target,
            send_sem=send,
            recv_sem=recv,
            device_id=device,
            device_id_type=pl.DeviceIdType.MESH,
        )

    def load(m, at):
        here = pl.ds(at * chunk, chunk)
        return pltpu.make_async_copy(routed_in[m].at[here], raw.at[m, here], load_sem.at[m])

    def loaded(m):
        pltpu.make_async_copy(routed_in[m], raw.at[m], load_sem.at[m]).wait()

    def load_shared(m):
        return pltpu.make_async_copy(shared_in[m], shared_raw.at[m], shared_load_sem.at[m])

    def to_peer(k, dst):
        return mesh_copy(
            packed[k].at[dst], held[k].at[me, core], send_sem.at[k], recv_sem.at[k, me], {"tp": dst}
        )

    def from_peer(k, src):
        return mesh_copy(
            packed[k].at[src], held[k].at[src, core], send_sem.at[k], recv_sem.at[k, src], {"tp": src}
        )

    def to_core(k, src, half):
        return mesh_copy(
            held[k].at[src, half],
            held[k].at[src, half],
            pass_send.at[k],
            pass_recv.at[k, src],
            {"fs": other},
        )

    def rim_copy(k):
        here = (pl.ds(0, 2), pl.ds(2, 1))[k]
        return mesh_copy(
            raw.at[here, pl.ds(0, edge * n)], rim.at[here], rim_sem.at[0, k], rim_sem.at[1, k], {"fs": other}
        )

    def shared_rim_copy():
        return mesh_copy(
            shared_raw.at[:, pl.ds(0, 8)], shared_rim, rim_sem.at[0, 2], rim_sem.at[1, 2], {"fs": other}
        )

    def shared_copy(half):
        return mesh_copy(
            shared_half.at[half], shared_half.at[half], shared_sem.at[0], shared_sem.at[1], {"fs": other}
        )

    def to_plane(a, b):
        return mesh_copy(
            parts.at[a, b],
            plane.at[a, my_b],
            plane_send.at[0],
            plane_recv.at[a],
            {"tp": my_a * inner + b},
        )

    def to_beside():
        return mesh_copy(
            stage.at[0], line.at[0], line_send.at[0], line_recv.at[0], {"tp": beside * inner + my_b}
        )

    def to_relay(k):
        return mesh_copy(
            stage.at[k + 1],
            relay.at[k],
            line_send.at[0],
            relay_recv.at[k],
            {"tp": beside * inner + my_b},
        )

    def to_line(k, a):
        return mesh_copy(
            stage.at[k + 1], line.at[1], line_send.at[0], line_recv.at[1], {"tp": a * inner + my_b}
        )

    def assemble(value, tail):
        cut = block - TILE
        body = jnp.where(first, value[0:cut], value[edge : cut + edge])
        rest = jnp.where(
            first,
            jnp.concatenate([value[cut:rows], tail[0:edge]], axis=0),
            jnp.concatenate(
                [value[cut + edge : rows], jnp.zeros((2 * edge, columns), jnp.float32)], axis=0
            ),
        )
        return cut, body, rest

    smalls = [
        pltpu.make_async_copy(source, target, small_sem.at[at])
        for at, (source, target) in enumerate(
            (
                (gain_in, gain_ref),
                (tokens_in, tokens_ref),
                (ids_in, ids_ref),
                (scores_in, scores_ref),
            )
        )
    ]
    smalls[0].start()
    for m in range(3):
        load_shared(m).start()
    for m in range(3):
        for at in range(chunks):
            load(m, at).start()
    for copy in smalls[1:]:
        copy.start()

    barrier = pltpu.get_barrier_semaphore()
    pl.semaphore_signal(
        barrier, inc=1, device_id={"fs": other}, device_id_type=pl.DeviceIdType.MESH
    )

    def greet(step, carry):
        pl.semaphore_signal(
            barrier,
            inc=1,
            device_id={"tp": (me + step) % n},
            device_id_type=pl.DeviceIdType.MESH,
        )
        return carry

    lax.fori_loop(1, n, greet, 0)
    smalls[0].wait()
    for m in range(3):
        load_shared(m).wait()
    loaded(0)
    loaded(1)
    pl.semaphore_wait(barrier, n)

    @pl.when(core == 1)
    def _():
        shared_rim_copy().start()
        rim_copy(0).start()

    @pl.when(core == 0)
    def _():
        shared_rim_copy().wait_recv()
        rim_copy(0).wait_recv()

    gain = gain_ref[...]
    for m in range(3):
        scale = gain if m < 2 else jnp.ones_like(gain)
        cut, body, rest = assemble(shared_raw[m], shared_rim[m])
        shared_half[core, m, 0:cut] = (body * scale).astype(jnp.bfloat16)
        shared_half[core, m, cut:block] = (rest * scale).astype(jnp.bfloat16)

    def pack(m, dst, target):
        scale = gain if m < 2 else jnp.ones_like(gain)
        cut = block - TILE
        start = dst + core * (edge * n)
        body = raw[m, pl.ds(start, cut, stride=n), :]
        end = raw[m, pl.ds(dst + cut * n, rows - cut, stride=n), :]
        head = rim[m, pl.ds(dst, edge, stride=n), :]
        rest = jnp.where(
            first,
            jnp.concatenate([end, head], axis=0),
            jnp.concatenate([end[edge:], jnp.zeros((2 * edge, columns), jnp.float32)], axis=0),
        )
        target[0:cut] = (body * scale).astype(jnp.bfloat16)
        target[cut:block] = (rest * scale).astype(jnp.bfloat16)
        target[block : block + piece] = shared_half[
            core, m, pl.ds(pl.multiple_of(dst * piece, TILE), piece)
        ]

    def pack_all(k, dst):
        if k == 0:
            for m in range(2):
                pack(m, dst, packed_pre.at[dst, m])
        else:
            pack(2, dst, packed_down.at[dst])

    def member(plane_at, shift):
        column = (my_b + shift) % 2 + 2 * ((my_b // 2 + shift // 2) % 2)
        return plane_at * inner + column

    def shift_of(k, step, rising):
        if k == 0:
            turn = step + rising * (inner - 1 - 2 * step)
            return (2 * turn + 1 - turn // 2) % inner
        return (1 + 2 * step + step // 2) % inner

    def peer_to(k, plane_at, step):
        return member(plane_at, shift_of(k, step, (plane_at > my_a).astype(jnp.int32)))

    def peer_from(k, plane_at, step):
        return member(plane_at, shift_of(k, step, (plane_at < my_a).astype(jnp.int32)))

    def peer_own(step):
        return member(my_a, step + 1)

    def send_plane(k, plane_at, start):
        def send(step, carry):
            dst = peer_to(k, plane_at, step)
            pack_all(k, dst)
            if start:
                to_peer(k, dst).start()
            return carry

        lax.fori_loop(0, inner, send, 0)

    def send_own(k):
        def send(step, carry):
            dst = peer_own(step)
            pack_all(k, dst)
            to_peer(k, dst).start()
            return carry

        lax.fori_loop(0, inner - 1, send, 0)

    def launch(k, plane_at):
        def send(step, carry):
            to_peer(k, peer_to(k, plane_at, step)).start()
            return carry

        lax.fori_loop(0, inner, send, 0)

    for plane_at in (mirror, skip, beside):
        send_plane(0, plane_at, True)
    send_own(0)
    loaded(2)

    @pl.when(core == 1)
    def _():
        rim_copy(1).start()

    @pl.when(core == 0)
    def _():
        rim_copy(1).wait_recv()

    send_plane(1, beside, True)
    send_own(1)
    for plane_at in (skip, mirror):
        send_plane(1, plane_at, False)

    @pl.when(inner_plane == 1)
    def _():
        launch(1, skip)
        launch(1, mirror)

    for m in range(2):
        pack(m, me, held_pre.at[me, core, m])
    pack(2, me, held_down.at[me, core])
    shared_copy(core).start()

    for copy in smalls[1:]:
        copy.wait()
    tokens = tokens_ref[...].astype(jnp.float32)
    mean = jnp.mean(tokens * tokens, axis=1, keepdims=True)
    scaled = (tokens * lax.rsqrt(mean + EPSILON)).astype(jnp.bfloat16)
    for i in range(n):
        normed[i] = scaled[:, i * columns : (i + 1) * columns]
    scores = scores_ref[...]
    weights = ROUTED_SCALE * scores / jnp.sum(scores, axis=0, keepdims=True)
    weight = jnp.sum(jnp.where(ids_ref[...] == me, weights, 0.0), axis=0, keepdims=True)
    weight = jnp.transpose(jnp.broadcast_to(weight, (8, weight.shape[1])))[:, 0:1]
    gate_acc[...] = jnp.zeros_like(gate_acc)
    up_acc[...] = jnp.zeros_like(up_acc)

    hidden = 2 * (block + piece)

    def arrive(k, src, local):
        if not local:
            from_peer(k, src).wait_recv()
        to_core(k, src, core).start()

    def add(src):
        to_core(0, src, other).wait_recv()
        for m, acc in ((0, gate_acc), (1, up_acc)):
            acc[...] += lax.dot_general(
                normed[src],
                held_pre[src, :, m].reshape(hidden, columns),
                (((1,), (1,)), ((), ())),
                preferred_element_type=jnp.float32,
            )

    def part(src):
        to_core(1, src, other).wait_recv()
        a, b = src // inner, src % inner
        parts[a, b] = jnp.dot(
            act[...], held_down[src].reshape(hidden, columns), preferred_element_type=jnp.float32
        ).astype(jnp.bfloat16)

        @pl.when(b != my_b)
        def _():
            to_plane(a, b).start()

    def stream(k, use, planes, after):
        arrive(k, me, True)
        before = me
        for at, plane_at in enumerate(planes):

            def one(step, waiting):
                src = peer_own(step) if at == 0 else peer_from(k, plane_at, step)
                arrive(k, src, False)
                use(waiting)
                return src

            before = lax.fori_loop(0, inner - 1 if at == 0 else inner, one, before)
            after(at)
        use(before)

    stream(0, add, (my_a, third, beside, fourth), lambda at: None)

    @pl.when(edge_plane == 1)
    def _():
        launch(1, mirror)
        launch(1, skip)

    gate_pre = gate_acc[...]
    place = lax.broadcasted_iota(jnp.int32, gate_pre.shape, 1) % (block + piece)
    share = jnp.where(place < block, weight, 1.0)
    act[...] = (gate_pre / (1.0 + jnp.exp(-gate_pre)) * up_acc[...] * share).astype(jnp.bfloat16)

    def plane_sum(a):
        mesh_copy(
            parts.at[a, pl.ds(0, inner - 1)],
            plane.at[a, pl.ds(0, inner - 1)],
            plane_send.at[0],
            plane_recv.at[a],
            {"fs": other},
        ).wait_recv()
        result = parts[a, my_b].astype(jnp.float32)
        for db in range(1, inner):
            result = result + plane[a, (my_b + db) % inner].astype(jnp.float32)
        return result

    def flush_beside():
        stage[0] = plane_sum(beside).astype(jnp.bfloat16)
        to_beside().start()

    def flush(k, a):
        summed[...] = plane_sum(a)

        @pl.when(edge_plane == 1)
        def _():
            stage[k + 1] = summed[...].astype(jnp.bfloat16)
            to_relay(k).start()

        @pl.when(inner_plane == 1)
        def _():
            to_relay(k).wait_recv()
            stage[k + 1] = (summed[...] + relay[k].astype(jnp.float32)).astype(jnp.bfloat16)
            to_line(k, a).start()

    stream(1, part, (my_a, beside, third), lambda at: None)

    def last(step, carry):
        src = peer_from(1, fourth, step)
        arrive(1, src, False)
        part(src)
        return carry

    lax.fori_loop(0, inner - 2, last, 0)
    flush_beside()
    lax.fori_loop(inner - 2, inner - 1, last, 0)
    flush(0, third)
    lax.fori_loop(inner - 1, inner, last, 0)
    flush(1, fourth)
    summed[...] = plane_sum(my_a)
    to_beside().wait_recv()
    summed[...] += line[0].astype(jnp.float32)
    shared_copy(other).wait_recv()
    to_line(0, my_a).wait_recv()
    mix[...] = (summed[...] + line[1].astype(jnp.float32)).astype(jnp.bfloat16)

    for k in range(2):
        mesh_copy(
            packed[k].at[pl.ds(0, n - 1)],
            packed[k].at[pl.ds(0, n - 1)],
            send_sem.at[k],
            recv_sem.at[k, 0],
            {"fs": other},
        ).wait_send()
        mesh_copy(
            held[k].at[:, core], held[k].at[:, core], pass_send.at[k], pass_recv.at[k, 0], {"fs": other}
        ).wait_send()

    @pl.when(core == 1)
    def _():
        shared_rim_copy().wait_send()
        rim_copy(0).wait_send()
        rim_copy(1).wait_send()

    shared_copy(core).wait_send()
    mesh_copy(
        parts.at[:, pl.ds(0, inner - 1)],
        plane.at[:, pl.ds(0, inner - 1)],
        plane_send.at[0],
        plane_recv.at[0],
        {"fs": other},
    ).wait_send()
    mesh_copy(stage, stage, line_send.at[0], line_recv.at[0], {"fs": other}).wait_send()


def store(
    n, block, held_pre, held_down, shared_half, mix, gate_out, up_out, down_out, sgate_out, sup_out, sdown_out, mix_out, sem
):
    columns = mix.shape[1]
    sizes = (block, gate_out.shape[0] - block)
    routed_out = (gate_out, up_out, down_out)
    shared_out = (sgate_out, sup_out, sdown_out)
    for m in range(3):
        for src in range(n):
            for half in range(2):
                source = held_down.at[src, half] if m == 2 else held_pre.at[src, half, m]
                pltpu.make_async_copy(
                    source.at[pl.ds(0, sizes[half])],
                    routed_out[m].at[pl.ds(half * block, sizes[half]), pl.ds(src * columns, columns)],
                    sem.at[m],
                ).start()
        for half in range(2):
            pltpu.make_async_copy(
                shared_half.at[half, m, pl.ds(0, sizes[half])],
                shared_out[m].at[pl.ds(half * block, sizes[half])],
                sem.at[3 + m],
            ).start()
    pltpu.make_async_copy(mix, mix_out, sem.at[6]).start()
    for at, target in enumerate((*routed_out, *shared_out, mix_out)):
        pltpu.make_async_copy(target, target, sem.at[at]).wait()


def on_device(n, shape, gate, up, down, sgate, sup, sdown, gain, tokens, ids, scores):
    block, edge, piece = shape
    experts, rows, columns = gate.shape
    count, width = tokens.shape
    unit = block + piece
    hidden = 2 * unit
    inner, outer = INNER, n // INNER
    sem = pltpu.SemaphoreType.DMA
    hbm = pl.BlockSpec(memory_space=pltpu.HBM)
    vmem = pl.BlockSpec(memory_space=pltpu.VMEM)
    bf16, f32 = jnp.bfloat16, jnp.float32
    results = pl.pallas_call(
        functools.partial(kernel, n, block, edge, piece),
        out_shape=(
            pltpu.VMEM((n, 2, 2, unit, columns), bf16),
            pltpu.VMEM((n, 2, unit, columns), bf16),
            pltpu.VMEM((2, 3, block, columns), bf16),
            pltpu.VMEM((count, columns), bf16),
        ),
        in_specs=[hbm] * 10,
        out_specs=(vmem,) * 4,
        scratch_shapes=[
            pltpu.VMEM((1, columns), f32),
            pltpu.VMEM(tokens.shape, bf16),
            pltpu.VMEM(ids.shape[::-1], jnp.int32),
            pltpu.VMEM(scores.shape[::-1], f32),
            pltpu.VMEM((3, n * rows, columns), f32),
            pltpu.VMEM((3, rows, columns), f32),
            pltpu.VMEM((3, n * edge, columns), f32),
            pltpu.VMEM((3, 8, columns), f32),
            pltpu.VMEM((n, 2, unit, columns), bf16),
            pltpu.VMEM((n, unit, columns), bf16),
            pltpu.VMEM((n, count, columns), bf16),
            pltpu.VMEM((count, hidden), f32),
            pltpu.VMEM((count, hidden), f32),
            pltpu.VMEM((count, hidden), bf16),
            pltpu.VMEM((outer, inner, count, columns), bf16),
            pltpu.VMEM((outer, inner, count, columns), bf16),
            pltpu.VMEM((count, columns), f32),
            pltpu.VMEM((3, count, columns), bf16),
            pltpu.VMEM((2, count, columns), bf16),
            pltpu.VMEM((2, count, columns), bf16),
            sem((4,)),
            sem((3,)),
            sem((3,)),
            sem((2, 3)),
            sem((2,)),
            sem((2,)),
            sem((2, n)),
            sem((2,)),
            sem((2, n)),
            sem((1,)),
            sem((outer,)),
            sem((1,)),
            sem((2,)),
            sem((2,)),
        ],
        compiler_params=pltpu.CompilerParams(
            collective_id=0, has_side_effects=True, vmem_limit_bytes=VMEM_BYTES
        ),
    )(
        *[
            pltpu.with_memory_space_constraint(array, pltpu.HBM)
            for array in (
                *[
                    jnp.transpose(array, (1, 0, 2)).reshape(rows * n, columns)
                    for array in (gate, up, down)
                ],
                sgate,
                sup,
                sdown,
                gain[None, :],
                tokens,
                ids.T,
                scores.T,
            )
        ]
    )
    full = jax.ShapeDtypeStruct((2 * rows, width), bf16)
    thin = jax.ShapeDtypeStruct((2 * rows, columns), bf16)
    whole = pl.pallas_call(
        functools.partial(store, n, block),
        out_shape=(full, full, full, thin, thin, thin, jax.ShapeDtypeStruct((count, columns), bf16)),
        in_specs=[vmem] * 4,
        out_specs=(hbm,) * 7,
        scratch_shapes=[sem((7,))],
        compiler_params=pltpu.CompilerParams(vmem_limit_bytes=VMEM_BYTES),
    )(*[pltpu.with_memory_space_constraint(array, pltpu.VMEM) for array in results])
    return (*[array[None] for array in whole[:3]], *whole[3:])


def body(n, n_fs, *args):
    experts, rows, columns = args[0].shape
    shape = geometry(n, n_fs, experts, rows, columns)
    if shape is None:
        return plain_on_device(*args)
    return on_device(n, shape, *args)


def solution(mesh):
    placed = (
        P(None, "fs", "tp"),
        P(None, "fs", "tp"),
        P(None, "fs", "tp"),
        P("fs", "tp"),
        P("fs", "tp"),
        P("fs", "tp"),
        P("tp"),
        P("fs", None),
        P("fs", None),
        P("fs", None),
    )
    return jax.shard_map(
        functools.partial(body, mesh.shape["tp"], mesh.shape["fs"]),
        mesh=mesh,
        in_specs=placed,
        out_specs=(
            P("tp", None, None),
            P("tp", None, None),
            P("tp", None, None),
            P(None, "tp"),
            P(None, "tp"),
            P(None, "tp"),
            P("fs", "tp"),
        ),
        check_vma=False,
    )
```

time: 99.5 us -> 92.4 us (0.929)
  Pallas kernels: 98.7 us -> 91.6 us
    pallas_call x1, Pallas kernels: 93 us -> 88.8 us  [on_device(): pl.pallas_call(functools.partial(kernel, n, block, edge, piece), out_shap...]
    pallas_call x1, Pallas kernels: 5.7 us -> 2.76 us  [on_device(): pl.pallas_call(functools.partial(store, n, block), out_shape=(full, full,...]
where the time goes in v2:
time: 92.4 us; the launch traced here: 92.2 us
  Pallas kernels  91.6 us (99%)
    pallas_call x1, Pallas kernels, on_device(): pl.pallas_call(functools.partial(kernel, n, block, edge, piece), out_shap...  88.8 us
    pallas_call x1, Pallas kernels, on_device(): pl.pallas_call(functools.partial(store, n, block), out_shape=(full, full,...  2.76 us

profile of v2, /device:TPU:8, one launch (start us, length us, event | category | flops | bytes accessed | tf_op | source)
XLA Modules:
  0.0 92.2 jit_solution(13234011688366754497)
XLA Ops:
  0.6 88.8 %shard_map.153 = (bf16[16,2,2,272,128]{4,3,2,1,0:T(8,128)(2,1)S(1)}, bf16[16,2,272,128]{3,2,1,0:T(8,128)(2,1)S(1)}, bf16[2,3,256,128]{3,2,1,0:T(8,128)(2,1)S(1)}, bf16[256,128]{1,0:T(8,128)(2,1)S(1)}) custom-call(f32[4032,128]{1,0:T(8,128)} %bitcast.15, f32[4032,128]{1,0:T(8,128)} %bitcast.16, f32[4032,128]{1,0:T(8,128)} %bitcast.17, f32[252,128]{1,0:T(8,128)} %sgate_in.1, ...), custom_call_target="tpu_custom_call" | custom-call | tf_op jit(solution)/shard_map/pallas_call | solution.py:639
  89.5 2.8 %shard_map.154 = (bf16[504,2048]{1,0:T(8,128)(2,1)}, bf16[504,2048]{1,0:T(8,128)(2,1)}, bf16[504,2048]{1,0:T(8,128)(2,1)}, bf16[504,128]{1,0:T(8,128)(2,1)}, bf1...) custom-call(bf16[16,2,2,272,128]{4,3,2,1,0:T(8,128)(2,1)S(1)} %get-tuple-element.18.held_pre, ...), custom_call_target="tpu_custom_call" | custom-call | tf_op jit(solution)/shard_map/pallas_call | solution.py:708
